TPU v7x, 128 devices: a 2x2x16 block of a 8x8x16 slice. The times are simulated.
128 devices in a mesh: grp: 4 (over y, x), tp: 32 (over z, core).
Axes of the slice: x: 2, y: 2, z: 16, core: 2. Of those that a mesh axis runs over, the one named last changes fastest.
The devices are a block of a 8x8x16 slice.
Arguments:
- tokens: bfloat16 [4096, 2048], P('grp', 'tp'), parts along dimension 0, may hold values from -8 to 8
- carried: float32 [2, 2, 32, 64, 4096], P(None, None, 'tp', None, 'grp'), parts along dimension 4, may hold values from -3 to 3
- proj_in: bfloat16 [2, 2048, 512], P(None, None, 'tp'), may hold values from -0.125 to 0.125
- proj_gate: bfloat16 [2, 2048, 512], P(None, None, 'tp'), may hold values from -0.125 to 0.125
- proj_out: bfloat16 [2, 512, 2048], P(None, None, 'tp'), may hold values from -0.5 to 0.5
- norm_params: bfloat16 [2, 2, 2048], P(None, None, 'tp'), may hold values from -0.5 to 2.4
- lambda_re: float32 [2, 32, 64], P(None, 'tp'), may hold values from -1 to -0.05
- lambda_im: float32 [2, 32, 64], P(None, 'tp'), may hold values from -3 to 3
- log_step: float32 [2, 32], P(None, 'tp'), may hold values from -3 to 0
- in_coupling: float32 [2, 2, 32, 64, 16], P(None, None, 'tp'), may hold values from -1 to 1
- out_coupling: float32 [2, 2, 32, 16, 64], P(None, None, 'tp'), may hold values from -1.5 to 1.5
- skip_gain: float32 [2, 512], P(None, 'tp'), may hold values from -4 to 4
Outputs:
- stream_out: bfloat16 [4096, 2048], P('grp', 'tp'), parts along dimension 0
- new_carried: float32 [2, 2, 32, 64, 4096], P(None, None, 'tp', None, 'grp'), parts along dimension 4
There are 4 independent parts, one for each index of `grp`. A program takes and returns all parts, laid end to end along the dimension named above; an argument that names none is the same for every part. Nothing has to cross between parts.
All inputs are finite; a program needn't handle non-finite values.
Results may differ from a plain program's by a relative error of at most 0.015.
Values may be sent and summed in bfloat16 or wider, within the bound.
A program may use at most 64 MiB of HBM per device.

v0:
```python
import jax
import jax.numpy as jnp
from jax import lax
from jax.sharding import Mesh
from jax.sharding import PartitionSpec as P

TP = ("tp_0", "tp_1")
residual_scale = 1.4142135623730951
norm_eps = 1e-05


def gather_turned(arrays, axis, dims):
    turned = [jnp.moveaxis(a, dim, 0) for a, dim in zip(arrays, dims)]
    both = jnp.concatenate([t.reshape(len(t), -1) for t in turned], axis=1)
    out, at, finished = (lax.all_gather(both, axis, axis=0, tiled=True), 0, [])
    for t, dim in zip(turned, dims):
        piece = out[:, at : at + t[0].size].reshape(-1, *t.shape[1:])
        finished.append(jnp.moveaxis(piece, 0, dim))
        at += t[0].size
    return tuple(finished)


def in_order(tiles, dim):
    tiles = jnp.moveaxis(tiles, 0, dim)
    shape = tiles.shape
    return tiles.reshape(*shape[:dim], shape[dim] * shape[dim + 1], *shape[dim + 2 :])


def all_blocks(array, axes, sequence):
    tiles = array
    for k in sequence:
        tiles = lax.all_gather(tiles, axes[k])
    done = sequence[::-1]
    back = [done.index(k) for k in range(len(axes))]
    tiles = tiles.transpose(*back, *range(len(axes), tiles.ndim))
    return tiles.reshape(-1, *array.shape)


def gather_axes(array, axes, sequence, dim):
    return in_order(all_blocks(array, axes, sequence), dim)


def discretize(lam_re, lam_im, log_dt, coupling):
    step_len = jnp.exp(log_dt)[:, None]
    modulus = jnp.exp(lam_re * step_len)
    decay_re = modulus * jnp.cos(lam_im * step_len)
    decay_im = modulus * jnp.sin(lam_im * step_len)
    denominator = lam_re * lam_re + lam_im * lam_im
    shifted = decay_re - 1.0
    coef_re = (shifted * lam_re + decay_im * lam_im) / denominator
    coef_im = (decay_im * lam_re - shifted * lam_im) / denominator
    in_re = coef_re[..., None] * coupling[0] - coef_im[..., None] * coupling[1]
    in_im = coef_re[..., None] * coupling[1] + coef_im[..., None] * coupling[0]
    return (decay_re, decay_im, in_re, in_im)


def recur(drive, gate_pre, states, lam_re, lam_im, log_dt, in_c, output_coupling, skip_connection):
    channel_groups = lam_re.shape[0]
    batch_rows = drive.shape[0]
    drive_expanded = drive.astype(jnp.float32).reshape(batch_rows, channel_groups, -1)
    decay_re, decay_im, in_re, in_im = discretize(lam_re, lam_im, log_dt, in_c)
    push_re = jnp.einsum("bgc,gpc->gpb", drive_expanded, in_re)
    push_im = jnp.einsum("bgc,gpc->gpb", drive_expanded, in_im)
    fresh_real = decay_re[..., None] * states[0] - decay_im[..., None] * states[1] + push_re
    fresh_imaginary = decay_re[..., None] * states[1] + decay_im[..., None] * states[0] + push_im
    readout_rows = (
        jnp.einsum("jyn,jmy->njm", fresh_real, output_coupling[0])
        - jnp.einsum("jyn,jmy->njm", fresh_imaginary, output_coupling[1])
        + skip_connection.reshape(channel_groups, -1) * drive_expanded
    )
    readout_rows = readout_rows.reshape(batch_rows, -1)
    gated = (jax.nn.gelu(readout_rows) * jax.nn.sigmoid(gate_pre.astype(jnp.float32))).astype(
        jnp.bfloat16
    )
    return (gated, jnp.stack([fresh_real, fresh_imaginary]))


def norm_whole(summed, params):
    wide = summed.astype(jnp.float32)
    mean_row = jnp.mean(wide, axis=-1, keepdims=True)
    var_row = jnp.mean(wide * wide, axis=-1, keepdims=True) - mean_row * mean_row
    scaled = (wide - mean_row) * lax.rsqrt(var_row + norm_eps)
    return (scaled * params[0].astype(jnp.float32) + params[1].astype(jnp.float32)).astype(
        jnp.bfloat16
    )


def per_device(
    tokens,
    carried,
    proj_in,
    proj_gate,
    proj_out,
    norm_params,
    lambda_re,
    lambda_im,
    log_step,
    in_coupling,
    out_coupling,
    skip_gain,
):
    layer_count = proj_in.shape[0]
    width_dev = tokens.shape[1]
    out_whole, params_whole = gather_turned((proj_out, norm_params), TP, (2, 2))
    whole_rows = lax.all_gather(tokens, TP, axis=1, tiled=True)
    new_states = []
    for layer_idx in range(layer_count):
        drive = jnp.dot(whole_rows, proj_in[layer_idx], preferred_element_type=jnp.float32).astype(
            jnp.bfloat16
        )
        gate_pre = jnp.dot(
            whole_rows, proj_gate[layer_idx], preferred_element_type=jnp.float32
        ).astype(jnp.bfloat16)
        gated, states = recur(
            drive,
            gate_pre,
            carried[layer_idx],
            lambda_re[layer_idx],
            lambda_im[layer_idx],
            log_step[layer_idx],
            in_coupling[layer_idx],
            out_coupling[layer_idx],
            skip_gain[layer_idx],
        )
        gated_all = gather_axes(gated, TP, (0, 1), 1)
        mixed = jnp.dot(gated_all, out_whole[layer_idx], preferred_element_type=jnp.float32)
        summed = (residual_scale * whole_rows.astype(jnp.float32) + mixed).astype(jnp.bfloat16)
        whole_rows = norm_whole(summed, params_whole[layer_idx])
        new_states.append(states)
    own_cols = lax.dynamic_slice_in_dim(whole_rows, lax.axis_index(TP) * width_dev, width_dev, 1)
    return (own_cols, jnp.stack(new_states))


def solution(mesh):
    finer = Mesh(mesh.devices.reshape(mesh.shape["grp"], 16, 2), ("grp", "tp_0", "tp_1"))
    return jax.shard_map(
        per_device,
        mesh=finer,
        in_specs=(
            P("grp", TP),
            P(None, None, TP, None, "grp"),
            P(None, None, TP),
            P(None, None, TP),
            P(None, None, TP),
            P(None, None, TP),
            P(None, TP, None),
            P(None, TP, None),
            P(None, TP),
            P(None, None, TP, None, None),
            P(None, None, TP, None, None),
            P(None, TP),
        ),
        out_specs=(P("grp", TP), P(None, None, TP, None, "grp")),
        check_vma=False,
    )
```

profile of v0, /device:TPU:69, one launch (start us, length us, event | category | flops | bytes accessed | tf_op | source)
XLA Modules:
  0.0 249.1 jit_solution(6978325671678053711)
XLA Ops:
  7.2 0.1 all-gather.9.cloned.1.call-start
  7.3 0.7 all-gather.9.cloned.1.call-update
  8.0 0.1 all-gather.11.cloned.1.call-start
  8.1 0.8 copy.43
  8.9 0.9 copy.54
  9.8 0.7 pad_maximum_fusion
  10.5 0.1 all-gather.13.cloned.1.call-start
  10.6 1.3 fusion.103
  13.3 0.8 slice_bitcast_fusion.4
  14.0 0.7 fusion.91
  14.8 0.8 fusion.97
  15.5 0.7 fusion.100
  16.2 71.2 %all-gather.9.cloned.1.call-done = bf16[1024,2048]{0,1:T(8,128)(2,1)} async-done(((bf16[1024,64]{0,1:T(8,128)(2,1)}), bf16[1024,2048]{0,1:T(8,128)(2,1)}) %all-gather.9.cloned.1.call-update) | async-done | bytes 4194320 | tf_op jit(solution)/shard_map/all_gather | solution.py:105
  87.4 3.0 %convolution_convert_fusion.1 = bf16[1024,16]{0,1:T(8,128)(2,1)S(1)} fusion(bf16[1024,2048]{0,1:T(8,128)(2,1)} %all-gather.9.cloned.1.call-done, bf16[2,2048,16]{1,2,0:T(8,128)(2,1)} %param.14), kind=kOutput, calls=%fused_computation.33 | convolution fusion | flops 67125248 | bytes 4292608 | tf_op jit(solution)/shard_map/dot_general | solution.py:108
  90.4 0.2 convolution_add_fusion.3
  90.6 0.1 fusion.64
  90.8 0.2 convolution_add_fusion.2
  91.0 0.2 fusion.40
  91.2 0.7 fusion.25
  91.9 27.8 %all-gather = bf16[16384,16]{0,1:T(8,128)(2,1)S(1)} all-gather(bf16[1024,16]{0,1:T(8,128)(2,1)S(1)} %fusion.25), channel_id=2, replica_groups=mesh['grp'=4,'tp_0'=16,'tp_1'=2] {'tp_0'}, dimensions={0}, use_global_device_ids=true | all-gather | bytes 557056 | tf_op jit(solution)/shard_map/all_gather | solution.py:32
  119.7 0.8 copy.58
  120.6 0.1 all-gather.15.cloned.1.call-start
  120.7 6.6 %copy.39 = bf16[1024,2048]{1,0:T(8,128)(2,1)} copy(bf16[1024,2048]{0,1:T(8,128)(2,1)} %all-gather.9.cloned.1.call-done) | data formatting | bytes 8388608 | tf_op jit(solution)/shard_map/all_gather | solution.py:105
  127.2 30.5 %all-gather.11.cloned.1.call-done = bf16[2048,1028]{1,0:T(8,128)(2,1)} async-done(((bf16[64,1028]{1,0:T(8,128)(2,1)}), bf16[2048,1028]{1,0:T(8,128)(2,1)}) %all-gather.11.cloned.1.call-update) | async-done | bytes 4210704 | tf_op jit(solution)/shard_map/all_gather | solution.py:15
  157.7 1.1 slice.178
  158.8 0.2 copy.45
  159.0 4.7 %slice.176 = bf16[2048,1024]{1,0:T(8,128)(2,1)} slice(bf16[2048,1028]{1,0:T(8,128)(2,1)} %all-gather.11.cloned.1.call-done), slice={[0:2048], [0:1024]} | slice | bytes 8388608 | tf_op jit(solution)/shard_map/slice | solution.py:17
  163.7 6.6 %copy.51 = bf16[2048,1024]{0,1:T(8,128)(2,1)} copy(bf16[2048,1024]{1,0:T(8,128)(2,1)} %slice.176) | data formatting | bytes 8388608 | tf_op jit(solution)/shard_map/reshape | solution.py:17
  170.3 3.0 %all-gather.13.cloned.1.call-done = bf16[32,1024,16]{1,2,0:T(8,128)(2,1)} async-done(((bf16[16,1024,16]{1,2,0:T(8,128)(2,1)}), bf16[32,1024,16]{1,2,0:T(8,128)(2,1)}) %all-gather.13.cloned.1.call-update) | async-done | bytes 1048592 | tf_op jit(solution)/shard_map/all_gather | solution.py:32
  173.3 1.3 copy.41
  174.6 6.0 %convert_reduce_fusion = (f32[1024]{0:T(1024)S(1)}, f32[1024]{0:T(1024)S(1)}, bf16[1024,2048]{1,0:T(8,128)(2,1)S(1)}) fusion(bf16[1024,512]{0,1:T(8,128)(2,1)S(1)} %bitcast.323, bf16[2,512,2048]{2,1,0:T(8,128)(2,1)} %bitcast.310, bf16[1024,2048]{1,0:T(8,128)(2,1)} %copy.39), kind=kOutput, calls=%fused_computation.2 | convolution fusion | flops 2164258816 | bytes 11542528 | tf_op jit(solution)/shard_map/dot_general | solution.py:126
  180.6 1.9 fusion.3
  182.5 1.2 convolution_convert_fusion.3
  183.7 0.2 convolution_add_fusion
  183.9 0.2 convolution_add_fusion.1
  184.2 0.1 fusion.57
  184.3 0.2 fusion.47
  184.4 1.2 fusion.24
  185.7 25.7 %all-gather.2 = bf16[16384,16]{0,1:T(8,128)(2,1)S(1)} all-gather(bf16[1024,16]{0,1:T(8,128)(2,1)S(1)} %fusion.24), channel_id=4, replica_groups=mesh['grp'=4,'tp_0'=16,'tp_1'=2] {'tp_0'}, dimensions={0}, use_global_device_ids=true | all-gather | bytes 557056 | tf_op jit(solution)/shard_map/all_gather | solution.py:32
  211.4 0.8 copy.57
  212.4 0.1 dynamic-slice
  212.4 0.1 dynamic-slice.1
  212.5 1.1 maximum_bitcast_fusion
  213.6 20.3 %all-gather.15.cloned.1.call-done = bf16[32,1024,16]{1,2,0:T(8,128)(2,1)} async-done(((bf16[16,1024,16]{1,2,0:T(8,128)(2,1)}), bf16[32,1024,16]{1,2,0:T(8,128)(2,1)}) %all-gather.15.cloned.1.call-update) | async-done | bytes 1048592 | tf_op jit(solution)/shard_map/all_gather | solution.py:32
  233.9 1.3 copy.47
  235.2 6.1 %fusion.102 = (f32[1024]{0:T(1024)S(1)}, f32[1024]{0:T(1024)S(1)}, f32[1024,2048]{1,0:T(8,128)S(1)}) fusion(bf16[1024,512]{0,1:T(8,128)(2,1)S(1)} %bitcast.322, bf16[2,512,2048]{2,1,0:T(8,128)(2,1)} %bitcast.311, bf16[1024,2048]{1,0:T(8,128)(2,1)} %copy-done), kind=kOutput, calls=%fused_computation.171 | convolution fusion | flops 2164258816 | bytes 15736832 | tf_op jit(solution)/shard_map/dot_general | solution.py:126
  241.3 0.5 fusion.29
  241.8 0.8 copy.49
  (23 shorter events, 0.3 us)
Async XLA Ops:
  7.2 83.2 %copy-start.5 = (f32[2,2,1,64,16]{3,4,2,1,0:T(8,128)S(1)}, f32[2,2,1,64,16]{3,4,2,1,0:T(8,128)}, u32[]{:S(2)}) copy-start(f32[2,2,1,64,16]{3,4,2,1,0:T(8,128)} %param.21) | copy-start | bytes 49156
  7.2 83.2 %copy-start.2 = (f32[2,2,1,64,1024]{4,3,2,1,0:T(8,128)S(1)}, f32[2,2,1,64,1024]{4,3,2,1,0:T(8,128)}, u32[]{:S(2)}) copy-start(f32[2,2,1,64,1024]{4,3,2,1,0:T(8,128)} %param.13) | copy-start | bytes 3145732
  7.2 83.4 %copy-start.6 = (f32[2,2,1,16,64]{4,3,2,1,0:T(8,128)S(1)}, f32[2,2,1,16,64]{4,3,2,1,0:T(8,128)}, u32[]{:S(2)}) copy-start(f32[2,2,1,16,64]{4,3,2,1,0:T(8,128)} %param.22) | copy-start | bytes 49156
  7.2 84.0 %copy-start.3 = (bf16[2,2048,16]{1,2,0:T(8,128)(2,1)S(1)}, bf16[2,2048,16]{1,2,0:T(8,128)(2,1)}, u32[]{:S(2)}) copy-start(bf16[2,2048,16]{1,2,0:T(8,128)(2,1)} %param.15) | copy-start | bytes 393220
  7.2 80.2 %all-gather.9.cloned.1.call-start = ((), (), s32[]{:S(2)}) async-start(), calls=%async_computation | async-start | bytes 4325376 | tf_op jit(solution)/shard_map/all_gather | solution.py:105
  8.0 149.7 %all-gather.11.cloned.1.call-start = ((), (), s32[]{:S(2)}) async-start(), calls=%async_computation.1 | async-start | bytes 4866048 | tf_op jit(solution)/shard_map/all_gather | solution.py:15
  10.5 162.8 %all-gather.13.cloned.1.call-start = ((), (), s32[]{:S(2)}) async-start(), calls=%async_computation.2 | async-start | bytes 1572864 | tf_op jit(solution)/shard_map/all_gather | solution.py:32
  87.4 3.8 %copy-start.1 = (bf16[1024,2048]{0,1:T(8,128)(2,1)S(1)}, bf16[1024,2048]{0,1:T(8,128)(2,1)}, u32[]{:S(2)}) copy-start(bf16[1024,2048]{0,1:T(8,128)(2,1)} %all-gather.9.cloned.1.call-done) | copy-start | bytes 12582916
  120.6 113.3 %all-gather.15.cloned.1.call-start = ((), (), s32[]{:S(2)}) async-start(), calls=%async_computation.3 | async-start | bytes 1572864 | tf_op jit(solution)/shard_map/all_gather | solution.py:32
  180.6 1.9 copy-start.4
  182.5 3.2 %copy-start = (bf16[1024,2048]{1,0:T(8,128)(2,1)}, bf16[1024,2048]{1,0:T(8,128)(2,1)S(1)}, u32[]{:S(2)}) copy-start(bf16[1024,2048]{1,0:T(8,128)(2,1)S(1)} %fusion.3) | copy-start | bytes 12582916
Sparse Core Ops, SparseCore 0:
  9.8 77.5 all-gather.8
  89.1 68.5 all-gather.10
  160.0 13.2 all-gather.12
  212.4 21.4 all-gather.14
where the time goes:
time: 250 us; the launch traced here: 249 us
  waiting for transfers between devices  126 us (50%)
  blocking collectives  53.5 us (21%)
  local copies, waits for them, and re-layouts  28.1 us (11%)
  matrix products  19.6 us (8%)
  between operations  15.4 us (6%)
  other arithmetic  6.37 us (3%)
    all_gather x1, waiting for transfers between devices, per_device(): whole_rows = lax.all_gather(tokens, TP, axis=1, tiled=True)  71.2 us
    all_gather x2, blocking collectives, all_blocks(): tiles = lax.all_gather(tiles, axes[k])  53.5 us
    all_gather x1, waiting for transfers between devices, gather_turned(): out, at, finished = (lax.all_gather(both, axis, axis=0, tiled=True), 0, [])  30.5 us
    all_gather x2, waiting for transfers between devices, all_blocks(): tiles = lax.all_gather(tiles, axes[k])  23.2 us
    dot_general x2, matrix products, per_device(): jnp.dot(gated_all, out_whole[layer_idx], preferred_element_type=jnp.float32)  12.1 us
    reshape x2, local copies, waits for them, and re-layouts, gather_turned(): piece = out[:, at:at + t[0].size].reshape(-1, *t.shape[1:])  6.58 us
    all_gather x1, local copies, waits for them, and re-layouts, per_device(): whole_rows = lax.all_gather(tokens, TP, axis=1, tiled=True)  6.56 us
    slice x3, local copies, waits for them, and re-layouts, gather_turned(): piece = out[:, at:at + t[0].size].reshape(-1, *t.shape[1:])  5.98 us
  transfers between devices with their start and end apart: 4, of which 4 were waited for; matrix products, arithmetic and copies ran while one was open for 13% of the time, Pallas kernels for 0%

commit v1 on v0

--- a/solution.py
+++ b/solution.py
@@ -102,7 +102,9 @@
     layer_count = proj_in.shape[0]
     width_dev = tokens.shape[1]
     out_whole, params_whole = gather_turned((proj_out, norm_params), TP, (2, 2))
-    whole_rows = lax.all_gather(tokens, TP, axis=1, tiled=True)
+    whole_rows = jnp.concatenate(
+        lax.all_to_all(jnp.stack([tokens] * lax.axis_size(TP)), TP, 0, 0), axis=1
+    )
     new_states = []
     for layer_idx in range(layer_count):
         drive = jnp.dot(whole_rows, proj_in[layer_idx], preferred_element_type=jnp.float32).astype(

time: 250 us -> 370 us (1.48)
  waiting for transfers between devices: 126 us -> 226 us
  starting transfers between devices: 0.25 us -> 18.9 us
    all_to_all x0 -> x1, waiting for transfers between devices: none -> 204 us  [per_device(): lax.all_to_all(jnp.stack([tokens] * lax.axis_size(TP)), TP, 0, 0)]
    all_gather x1 -> x0, waiting for transfers between devices: 71.2 us -> none  [per_device(): whole_rows = lax.all_gather(tokens, TP, axis=1, tiled=True)]
    all_gather x1, waiting for transfers between devices: 30.5 us -> 0.02 us  [gather_turned(): out, at, finished = (lax.all_gather(both, axis, axis=0, tiled=True), 0, [])]
    all_to_all x0 -> x1, starting transfers between devices: none -> 18.7 us  [per_device(): lax.all_to_all(jnp.stack([tokens] * lax.axis_size(TP)), TP, 0, 0)]
    reshape x0 -> x1, local copies, waits for them, and re-layouts: none -> 6.68 us  [per_device(): jnp.concatenate(lax.all_to_all(jnp.stack([tokens] * lax.axis_size(TP)), T...]
    all_gather x1 -> x0, local copies, waits for them, and re-layouts: 6.56 us -> none  [per_device(): whole_rows = lax.all_gather(tokens, TP, axis=1, tiled=True)]
  transfers between devices with their start and end apart: 4 -> 4, of which waited for: 4 -> 2; matrix products, arithmetic and copies ran while one was open for 13% -> 8% of each run, Pallas kernels for 0% -> 0%
where the time goes in v1:
time: 370 us
  waiting for transfers between devices  226 us (61%)
  blocking collectives  54.6 us (15%)
  local copies, waits for them, and re-layouts  28.7 us (8%)
  matrix products  21.6 us (6%)
  starting transfers between devices  18.9 us (5%)
  between operations  15.5 us (4%)
  other arithmetic  4.34 us (1%)
    all_to_all x1, waiting for transfers between devices, per_device(): lax.all_to_all(jnp.stack([tokens] * lax.axis_size(TP)), TP, 0, 0)  204 us
    all_gather x2, blocking collectives, all_blocks(): tiles = lax.all_gather(tiles, axes[k])  54.6 us
    all_gather x2, waiting for transfers between devices, all_blocks(): tiles = lax.all_gather(tiles, axes[k])  22.4 us
    all_to_all x1, starting transfers between devices, per_device(): lax.all_to_all(jnp.stack([tokens] * lax.axis_size(TP)), TP, 0, 0)  18.7 us
    dot_general x2, matrix products, per_device(): jnp.dot(gated_all, out_whole[layer_idx], preferred_element_type=jnp.float32)  12.1 us
  transfers between devices with their start and end apart: 4, of which 2 were waited for; matrix products, arithmetic and copies ran while one was open for 8% of the time, Pallas kernels for 0%

profile of v1, /device:TPU:69, one launch (start us, length us, event | category | flops | bytes accessed | tf_op | source)
XLA Modules:
  0.0 369.8 jit_solution(17411419499256291668)
XLA Ops:
  7.2 3.5 stack.20
  10.7 0.0 copy-start.3
  10.7 18.7 %all-to-all-start = ((bf16[32,1024,64]{1,2,0:T(8,128)(2,1)}), bf16[32,1024,64]{1,2,0:T(8,128)(2,1)}, u32[]{:S(2)}, u32[]{:S(2)}) async-start(bf16[32,1024,64]{1,2,0:T(8,128)(2,1)} %stack.20), calls=%async_computation | async-start | bytes 8388608 | tf_op jit(solution)/shard_map/all_to_all | solution.py:106
  29.4 0.0 copy-start.1
  29.4 0.1 all-gather.8.cloned.1.call-start
  29.5 0.1 copy.43
  29.7 0.7 pad_maximum_fusion
  30.3 0.1 all-gather.8.cloned.1.call-update
  30.4 0.1 all-gather.10.cloned.1.call-start
  30.5 0.6 fusion.103
  32.5 0.1 fusion.97
  32.6 203.6 %all-to-all-done = bf16[32,1024,64]{1,2,0:T(8,128)(2,1)} async-done(((bf16[32,1024,64]{1,2,0:T(8,128)(2,1)}), bf16[32,1024,64]{1,2,0:T(8,128)(2,1)}, u32[]{:S(2)}, u32[]{:S(2)}) %all-to-all-start) | async-done | bytes 4194336 | tf_op jit(solution)/shard_map/all_to_all | solution.py:106
  236.2 2.8 convolution_convert_fusion.1
  239.1 0.2 convolution_add_fusion.3
  239.3 0.1 fusion.64
  239.5 0.2 convolution_add_fusion.2
  239.7 0.2 fusion.40
  239.9 2.9 fusion.25
  242.7 29.0 %all-gather = bf16[16384,16]{0,1:T(8,128)(2,1)S(1)} all-gather(bf16[1024,16]{0,1:T(8,128)(2,1)S(1)} %fusion.25), channel_id=2, replica_groups=mesh['grp'=4,'tp_0'=16,'tp_1'=2] {'tp_0'}, dimensions={0}, use_global_device_ids=true | all-gather | bytes 557056 | tf_op jit(solution)/shard_map/all_gather | solution.py:32
  271.7 0.8 copy.58
  272.6 0.1 all-gather.10.cloned.1.call-update
  272.6 0.1 all-gather.12.cloned.1.call-start
  272.7 0.0 all-gather.8.cloned.1.call-done
  272.7 1.1 slice.178
  273.8 0.2 copy.45
  274.0 4.7 %slice.176 = bf16[2048,1024]{1,0:T(8,128)(2,1)} slice(bf16[2048,1028]{1,0:T(8,128)(2,1)} %all-gather.8.cloned.1.call-done), slice={[0:2048], [0:1024]} | slice | bytes 8388608 | tf_op jit(solution)/shard_map/slice | solution.py:17
  278.7 6.5 %copy.51 = bf16[2048,1024]{0,1:T(8,128)(2,1)} copy(bf16[2048,1024]{1,0:T(8,128)(2,1)} %slice.176) | data formatting | bytes 8388608 | tf_op jit(solution)/shard_map/reshape | solution.py:17
  285.3 6.7 %copy.39 = bf16[1024,2048]{1,0:T(8,128)(2,1)} copy(bf16[1024,2048]{0,1:T(8,128)(2,1)} %bitcast.1) | data formatting | bytes 8388608 | tf_op jit(solution)/shard_map/reshape | solution.py:105
  292.0 1.3 copy.41
  293.3 6.0 %convert_reduce_fusion = (f32[1024]{0:T(1024)S(1)}, f32[1024]{0:T(1024)S(1)}, bf16[1024,2048]{1,0:T(8,128)(2,1)S(1)}) fusion(bf16[1024,512]{0,1:T(8,128)(2,1)S(1)} %bitcast.326, bf16[2,512,2048]{2,1,0:T(8,128)(2,1)} %bitcast.313, bf16[1024,2048]{1,0:T(8,128)(2,1)} %copy.39), kind=kOutput, calls=%fused_computation.2 | convolution fusion | flops 2164258816 | bytes 11542528 | tf_op jit(solution)/shard_map/dot_general | solution.py:128
  299.3 1.9 fusion.3
  301.2 1.2 convolution_convert_fusion.3
  302.4 0.2 convolution_add_fusion
  302.6 0.2 convolution_add_fusion.1
  302.8 0.1 fusion.57
  303.0 0.2 fusion.47
  303.1 1.2 fusion.24
  304.4 25.6 %all-gather.2 = bf16[16384,16]{0,1:T(8,128)(2,1)S(1)} all-gather(bf16[1024,16]{0,1:T(8,128)(2,1)S(1)} %fusion.24), channel_id=4, replica_groups=mesh['grp'=4,'tp_0'=16,'tp_1'=2] {'tp_0'}, dimensions={0}, use_global_device_ids=true | all-gather | bytes 557056 | tf_op jit(solution)/shard_map/all_gather | solution.py:32
  329.9 0.8 copy.57
  330.8 0.1 all-gather.12.cloned.1.call-update
  330.8 0.1 dynamic-slice
  330.9 0.1 dynamic-slice.1
  331.1 1.1 maximum_bitcast_fusion
  332.2 22.4 %all-gather.12.cloned.1.call-done = bf16[32,1024,16]{1,2,0:T(8,128)(2,1)} async-done(((bf16[16,1024,16]{1,2,0:T(8,128)(2,1)}), bf16[32,1024,16]{1,2,0:T(8,128)(2,1)}) %all-gather.12.cloned.1.call-update) | async-done | bytes 1048592 | tf_op jit(solution)/shard_map/all_gather | solution.py:32
  354.5 1.3 copy.47
  355.8 6.1 %fusion.102 = (f32[1024]{0:T(1024)S(1)}, f32[1024]{0:T(1024)S(1)}, f32[1024,2048]{1,0:T(8,128)S(1)}) fusion(bf16[1024,512]{0,1:T(8,128)(2,1)S(1)} %bitcast.325, bf16[2,512,2048]{2,1,0:T(8,128)(2,1)} %bitcast.314, bf16[1024,2048]{1,0:T(8,128)(2,1)} %copy-done), kind=kOutput, calls=%fused_computation.171 | convolution fusion | flops 2164258816 | bytes 15736832 | tf_op jit(solution)/shard_map/dot_general | solution.py:128
  361.9 0.5 fusion.29
  362.4 0.8 copy.49
  (33 shorter events, 0.3 us)
Async XLA Ops:
  10.7 18.8 %copy-start.10 = (bf16[2,2,64]{2,1,0:T(2,128)(2,1)S(1)}, bf16[2,2,64]{2,1,0:T(2,128)(2,1)}, u32[]{:S(2)}) copy-start(bf16[2,2,64]{2,1,0:T(2,128)(2,1)} %param.17) | copy-start | bytes 1540
  10.7 19.0 %copy-start.4 = (bf16[2,512,64]{1,2,0:T(8,128)(2,1)S(1)}, bf16[2,512,64]{1,2,0:T(8,128)(2,1)}, u32[]{:S(2)}) copy-start(bf16[2,512,64]{1,2,0:T(8,128)(2,1)} %param.16) | copy-start | bytes 393220
  10.7 19.8 %copy-start.9 = (f32[2,1]{0,1:T(1,128)S(1)}, f32[2,1]{0,1:T(1,128)}, u32[]{:S(2)}) copy-start(f32[2,1]{0,1:T(1,128)} %param.20) | copy-start | bytes 28
  10.7 21.8 %copy-start.11 = (f32[2,16]{1,0:T(2,128)S(1)}, f32[2,16]{1,0:T(2,128)}, u32[]{:S(2)}) copy-start(f32[2,16]{1,0:T(2,128)} %param.23) | copy-start | bytes 388
  10.7 21.8 %copy-start.7 = (f32[2,1,64]{2,1,0:T(1,128)S(1)}, f32[2,1,64]{2,1,0:T(1,128)}, u32[]{:S(2)}) copy-start(f32[2,1,64]{2,1,0:T(1,128)} %param.19) | copy-start | bytes 1540
  10.7 21.8 %copy-start.8 = (f32[2,1,64]{2,1,0:T(1,128)S(1)}, f32[2,1,64]{2,1,0:T(1,128)}, u32[]{:S(2)}) copy-start(f32[2,1,64]{2,1,0:T(1,128)} %param.18) | copy-start | bytes 1540
  10.7 225.5 %copy-start.3 = (bf16[2,2048,16]{1,2,0:T(8,128)(2,1)S(1)}, bf16[2,2048,16]{1,2,0:T(8,128)(2,1)}, u32[]{:S(2)}) copy-start(bf16[2,2048,16]{1,2,0:T(8,128)(2,1)} %param.14) | copy-start | bytes 393220
  10.7 225.5 %all-to-all-start = ((bf16[32,1024,64]{1,2,0:T(8,128)(2,1)}), bf16[32,1024,64]{1,2,0:T(8,128)(2,1)}, u32[]{:S(2)}, u32[]{:S(2)}) async-start(bf16[32,1024,64]{1,2,0:T(8,128)(2,1)} %stack.20), calls=%async_computation | async-start | bytes 8388608 | tf_op jit(solution)/shard_map/all_to_all | solution.py:106
  29.4 209.7 %copy-start.1 = (f32[2,2,1,64,1024]{4,3,2,1,0:T(8,128)S(1)}, f32[2,2,1,64,1024]{4,3,2,1,0:T(8,128)}, u32[]{:S(2)}) copy-start(f32[2,2,1,64,1024]{4,3,2,1,0:T(8,128)} %param.13) | copy-start | bytes 3145732
  29.4 209.7 %copy-start.5 = (f32[2,2,1,64,16]{3,4,2,1,0:T(8,128)S(1)}, f32[2,2,1,64,16]{3,4,2,1,0:T(8,128)}, u32[]{:S(2)}) copy-start(f32[2,2,1,64,16]{3,4,2,1,0:T(8,128)} %param.21) | copy-start | bytes 49156
  29.4 209.9 %copy-start.6 = (f32[2,2,1,16,64]{4,3,2,1,0:T(8,128)S(1)}, f32[2,2,1,16,64]{4,3,2,1,0:T(8,128)}, u32[]{:S(2)}) copy-start(f32[2,2,1,16,64]{4,3,2,1,0:T(8,128)} %param.22) | copy-start | bytes 49156
  29.4 210.4 %copy-start.2 = (bf16[2,2048,16]{1,2,0:T(8,128)(2,1)S(1)}, bf16[2,2048,16]{1,2,0:T(8,128)(2,1)}, u32[]{:S(2)}) copy-start(bf16[2,2048,16]{1,2,0:T(8,128)(2,1)} %param.15) | copy-start | bytes 393220
  29.4 243.3 %all-gather.8.cloned.1.call-start = ((), (), s32[]{:S(2)}) async-start(), calls=%async_computation.1 | async-start | bytes 4866048 | tf_op jit(solution)/shard_map/all_gather | solution.py:15
  30.4 261.6 %all-gather.10.cloned.1.call-start = ((), (), s32[]{:S(2)}) async-start(), calls=%async_computation.2 | async-start | bytes 1572864 | tf_op jit(solution)/shard_map/all_gather | solution.py:32
  272.6 81.9 %all-gather.12.cloned.1.call-start = ((), (), s32[]{:S(2)}) async-start(), calls=%async_computation.3 | async-start | bytes 1572864 | tf_op jit(solution)/shard_map/all_gather | solution.py:32
  301.2 3.2 copy-start
Sparse Core Ops, SparseCore 0:
  32.0 155.4 all-gather.7
  272.7 18.9 all-gather.9
  331.0 23.5 all-gather.11
